TPU v7x, 32 devices: a whole 2x2x4 slice. The times are simulated.
32 devices in a mesh: grp: 2 (over y), sp: 4 (over z), tp: 4 (over x, core).
Axes of the slice: x: 2, y: 2, z: 4, core: 2. Of those that a mesh axis runs over, the one named last changes fastest.
Arguments:
- queries: bfloat16 [1024, 2048], P(('grp', 'sp'), 'tp'), parts along dimension 0, may hold values from -8 to 8
- keys: bfloat16 [1024, 1024], P(('grp', 'sp'), 'tp'), parts along dimension 0, may hold values from -6 to 6
- values: bfloat16 [1024, 1024], P(('grp', 'sp'), 'tp'), parts along dimension 0, may hold values from -6 to 6
- head_bias: float32 [16], P('tp'), may hold values from -15 to -5
- documents: int32 [1024], P(('grp', 'sp')), parts along dimension 0, may hold values from 0 to 2, never falling along the last dimension, each value on 1 to 384 neighbouring positions
- w_out: bfloat16 [2048, 2048], P('tp'), may hold values from -0.125 to 0.125
- resid: bfloat16 [1024, 2048], P(('grp', 'sp', 'tp')), parts along dimension 0, may hold values from -6 to 6
- norm_gain: float32 [2048], replicated, may hold values from 0.1 to 1.9
- expert_ids: int32 [1024, 2], P(('grp', 'sp', 'tp')), parts along dimension 0, may hold values from 0 to 3, all different within a row; in each aligned block of 32 rows (0 to 31, 32 to 63, ...) at most 32 rows name the same one
- expert_gates: float32 [1024, 2], P(('grp', 'sp', 'tp')), parts along dimension 0, may hold values from 0.1 to 0.9
- w_gate: bfloat16 [4, 2048, 3072], P('sp', None, 'tp'), may hold values from -0.125 to 0.125
- w_up: bfloat16 [4, 2048, 3072], P('sp', None, 'tp'), may hold values from -0.125 to 0.125
- w_down: bfloat16 [4, 3072, 2048], P('sp', 'tp'), may hold values from -0.109375 to 0.109375
Outputs:
- layer_out: bfloat16 [1024, 2048], P(('grp', 'sp', 'tp')), parts along dimension 0
There are 2 independent parts, one for each index of `grp`. A program takes and returns all parts, laid end to end along the dimension named above; an argument that names none is the same for every part. Nothing has to cross between parts.
Inputs may be any that keep to these rules, and one draw needn't show every extreme that they name: Document numbers never fall along the sequence; each of the 3 documents holds at least one position and the longest exactly 384 positions. `expert_ids`: each position names 2 different experts. Among the 32 positions of one device (aligned blocks of 32 rows) no expert is named more than 32 times, and in some block some expert exactly 32 times.
All inputs are finite; a program needn't handle non-finite values.
Results may differ from a plain program's by a relative error of at most 0.012.
Values may be sent and summed in bfloat16 or wider, within the bound.
A program may use at most 64 MiB of HBM per device.

v0:
```python
import jax
import jax.numpy as jnp
from jax import lax
from jax.sharding import PartitionSpec as P

D = 2048
HEADS = 16
KV_HEADS = 8
DH = 128
TOPK = 2


def passed_along(value, axis, steps):
    count = lax.axis_size(axis)
    initial, last = (max(0, -steps), min(count, count - steps))
    return lax.ppermute(value, axis, [(source, source + steps) for source in range(initial, last)])


def attend_terms(query_grid, bias_grid, key_block, value_block, live, carried):
    kv_local = bias_grid.shape[0]
    key_count = key_block.shape[0]
    logits = (
        jnp.einsum(
            "qgrd,sgd->grqs",
            query_grid,
            key_block.reshape(key_count, kv_local, DH),
            preferred_element_type=jnp.float32,
        )
        * DH ** (-0.5)
        + bias_grid[:, :, None, None]
    )
    keep = jnp.where(live, jax.nn.log_sigmoid(-logits), 0.0)
    after = lax.cumsum(keep, axis=3, reverse=True) - keep + carried[:, :, :, None]
    weight = jnp.where(live, jnp.exp(jax.nn.log_sigmoid(logits) + after), 0.0).astype(jnp.bfloat16)
    partial_mix = jnp.einsum(
        "grqs,sgd->qgrd",
        weight,
        value_block.reshape(key_count, kv_local, DH),
        preferred_element_type=jnp.float32,
    )
    return (partial_mix, jnp.sum(keep, axis=3))


def local(
    queries,
    keys,
    values,
    head_bias,
    documents,
    w_out,
    resid,
    norm_gain,
    expert_ids,
    expert_gates,
    w_gate,
    w_up,
    w_down,
):
    tok_count = queries.shape[0]
    kv_local = keys.shape[1] // DH
    group_size = HEADS // KV_HEADS
    sp_count = lax.axis_size("sp")
    tp_count = lax.axis_size("tp")
    sp_index = lax.axis_index("sp")
    query_grid = queries.reshape(tok_count, kv_local, group_size, DH)
    bias_grid = head_bias.reshape(kv_local, group_size)
    doc_here = documents.astype(jnp.bfloat16)
    doc_column = doc_here.reshape(tok_count, 1)
    local_pos = jnp.arange(tok_count, dtype=jnp.int32)
    live_local = (local_pos[None, :] < local_pos[:, None]) & (
        documents[None, :] == documents[:, None]
    )
    zero_carry = jnp.zeros((kv_local, group_size, tok_count), jnp.float32)
    mix_total, carried = attend_terms(query_grid, bias_grid, keys, values, live_local, zero_carry)

    def visit(turn_index, state):
        mix_sum, carry_sum, key_block, value_block, doc_block = state
        key_block, value_block, doc_block = passed_along(
            (key_block, value_block, doc_block), "sp", 1
        )
        live = (doc_block[:, 0][None, :] == doc_here[:, None]) & (sp_index - turn_index >= 0)
        partial_mix, block_keep = attend_terms(
            query_grid, bias_grid, key_block, value_block, live, carry_sum
        )
        return (mix_sum + partial_mix, carry_sum + block_keep, key_block, value_block, doc_block)

    mix_total, carried, key_last, value_last, doc_last = lax.fori_loop(
        1, sp_count, visit, (mix_total, carried, keys, values, doc_column)
    )
    mixed = mix_total.reshape(tok_count, kv_local * group_size * DH).astype(jnp.bfloat16)
    projected = lax.psum_scatter(
        jnp.dot(mixed, w_out, preferred_element_type=jnp.float32).astype(jnp.bfloat16),
        "tp",
        scatter_dimension=0,
        tiled=True,
    ).astype(jnp.float32)
    middle = (resid.astype(jnp.float32) + projected).astype(jnp.bfloat16)
    middle_value = middle.astype(jnp.float32)
    normed = (
        middle_value
        * lax.rsqrt(jnp.mean(middle_value * middle_value, axis=1, keepdims=True) + 1e-06)
        * norm_gain
    ).astype(jnp.bfloat16)
    row_count = normed.shape[0]
    expert_count = w_gate.shape[0] * sp_count
    slot_limit = min(row_count, max(2, 2 * TOPK * row_count // expert_count))
    flat_ids = expert_ids.reshape(-1)
    onehot_ids = (flat_ids[:, None] == jnp.arange(expert_count, dtype=jnp.int32)[None, :]).astype(
        jnp.int32
    )
    earlier = jnp.cumsum(onehot_ids, axis=0) - onehot_ids
    slot_ids = jnp.sum(earlier * onehot_ids, axis=1)
    target = flat_ids * slot_limit + slot_ids
    placing = (
        jnp.arange(expert_count * slot_limit, dtype=jnp.int32)[:, None] == target[None, :]
    ).astype(jnp.bfloat16)
    by_token = jnp.sum(placing.reshape(expert_count * slot_limit, row_count, TOPK), axis=2)
    outgoing = jnp.dot(by_token, normed, preferred_element_type=jnp.float32).astype(jnp.bfloat16)
    outgoing = outgoing.reshape(expert_count, slot_limit, D)
    arrived = lax.all_to_all(outgoing, "sp", split_axis=0, concat_axis=0, tiled=True)
    gathered = lax.all_gather(arrived, "tp", axis=0, tiled=True)
    expert_rows = gathered.reshape(-1, D)
    gate_value = jnp.dot(expert_rows, w_gate[0], preferred_element_type=jnp.float32)
    up_value = jnp.dot(expert_rows, w_up[0], preferred_element_type=jnp.float32)
    hidden = (jax.nn.silu(gate_value) * up_value).astype(jnp.bfloat16)
    partial_out = jnp.dot(hidden, w_down[0], preferred_element_type=jnp.float32)
    summed = lax.psum_scatter(
        partial_out.reshape(tp_count, sp_count * slot_limit, D).astype(jnp.bfloat16),
        "tp",
        scatter_dimension=0,
        tiled=True,
    ).astype(jnp.float32)
    expert_result = summed.reshape(sp_count, slot_limit, D).astype(jnp.bfloat16)
    returned = lax.all_to_all(expert_result, "sp", split_axis=0, concat_axis=0, tiled=True)
    routed = jnp.dot(placing.T, returned.reshape(-1, D), preferred_element_type=jnp.float32)
    combined = jnp.sum(expert_gates[:, :, None] * routed.reshape(row_count, TOPK, D), axis=1)
    return (middle_value + combined).astype(jnp.bfloat16)


def solution(mesh):
    return jax.shard_map(
        local,
        mesh=mesh,
        in_specs=(
            P(("grp", "sp"), "tp"),
            P(("grp", "sp"), "tp"),
            P(("grp", "sp"), "tp"),
            P("tp"),
            P(("grp", "sp")),
            P("tp", None),
            P(("grp", "sp", "tp"), None),
            P(),
            P(("grp", "sp", "tp"), None),
            P(("grp", "sp", "tp"), None),
            P("sp", None, "tp"),
            P("sp", None, "tp"),
            P("sp", "tp", None),
        ),
        out_specs=P(("grp", "sp", "tp"), None),
        check_vma=False,
    )
```

profile of v0, /device:TPU:0, one launch (start us, length us, event | category | flops | bytes accessed | tf_op | source)
XLA Modules:
  0.0 232.2 jit_solution(13194715823110891600)
XLA Ops:
  17.9 2.4 %fusion.56 = (f32[2,2,128]{2,1,0:T(2,128)}, f32[2,2,128,128]{2,3,1,0:T(8,128)S(1)}, f32[2,2,128,128]{2,3,1,0:T(8,128)}) fusion(pred[128,128]{0,1:T(8,128)(4,1)S(1)} %fusion.50, f32[2,2]{1,0:T(2,128)} %add.157, bf16[128,2,2,128]{0,3,2,1:T(8,128)(2,1)S(1)} %bitcast.78, bf16[128,2,128,1]{2,1,0,3:T(2,128)(2,1)} %bitcast.81), kind=kOutput, calls=%fused_computation.74 | convolution fusion | flops 17497600 | bytes 739344 | tf_op jit(solution)/shard_map/qgrd,sgd->grqs/dot_general | solution.py:23
  20.3 5.1 %reduce_window_sum.31 = f32[2,2,128,128]{2,3,1,0:T(8,128)} reduce-window(f32[2,2,128,128]{2,3,1,0:T(8,128)S(1)} %get-tuple-element.239, f32[]{:T(128)} %constant.57.clone.1), window={size=1x1x1x128 pad=0_0x0_0x0_0x0_127}, to_apply=%region_0.1 | reduce-window | flops 8323072 | bytes 524292 | tf_op jit(solution)/shard_map/attend_terms/reduce_window_sum | solution.py:33
  27.7 69.8 %while.21 = (s32[]{:T(128)}, f32[128,2,2,128]{3,0,2,1:T(8,128)}, f32[2,2,128]{2,1,0:T(2,128)}, bf16[128,256]{0,1:T(8,128)(2,1)}, bf16[128,256]{0,1:T(8,128)(2,1)...) while((s32[]{:T(128)}, f32[128,2,2,128]{3,0,2,1:T(8,128)}, ...), condition=%wide.region_5.6_spmd, body=%wide.region_2.5_spmd.sunk | while | flops 44105732 | bytes 3207487 | solution.py:87
  27.7 4.9 %collective-permute-start.1 = (bf16[128,1]{0,1:T(2,128)(2,1)}, bf16[128,1]{0,1:T(2,128)(2,1)S(1)}, u32[]{:S(2)}, u32[]{:S(2)}) collective-permute-start(bf16[128,1]{0,1:T(2,128)(2,1)} %get-tuple-element.328), channel_id=1, source_target_pairs={{0,4},{4,8},{8,12},{1,5},{5,9},{9,13},{2,6},{6,10},{10,14},{3,7},{... | collective-permute-start | bytes 776 | tf_op jit(solution)/shard_map/while/body/eval_jaxpr/ppermute | solution.py:16
  32.7 3.5 %collective-permute-start.2 = (bf16[128,256]{0,1:T(8,128)(2,1)}, bf16[128,256]{0,1:T(8,128)(2,1)S(1)}, u32[]{:S(2)}, u32[]{:S(2)}) collective-permute-start(bf16[128,256]{0,1:T(8,128)(2,1)} %get-tuple-element.326), channel_id=1, source_target_pairs={{0,4},{4,8},{8,12},{1,5},{5,9},{9,13},{2,6},{6,10},{10,14},{3,7},{... | collective-permute-start | bytes 196616 | tf_op jit(solution)/shard_map/while/body/eval_jaxpr/ppermute | solution.py:16
  36.2 3.5 %collective-permute-start = (bf16[128,256]{0,1:T(8,128)(2,1)}, bf16[128,256]{0,1:T(8,128)(2,1)S(1)}, u32[]{:S(2)}, u32[]{:S(2)}) collective-permute-start(bf16[128,256]{0,1:T(8,128)(2,1)} %get-tuple-element.327), channel_id=1, source_target_pairs={{0,4},{4,8},{8,12},{1,5},{5,9},{9,13},{2,6},{6,10},{10,14},{3,7},{... | collective-permute-start | bytes 196616 | tf_op jit(solution)/shard_map/while/body/eval_jaxpr/ppermute | solution.py:16
  41.7 2.6 %fusion.80 = (f32[2,2,128]{2,1,0:T(2,128)}, f32[2,2,128,128]{2,3,1,0:T(8,128)}, f32[2,2,128,128]{2,3,1,0:T(8,128)}) fusion(pred[128,128]{0,1:T(8,128)(4,1)S(1)} %compare_and_fusion.2, f32[2,2]{1,0:T(2,128)S(1)} %add.252, bf16[128,2,128,1]{0,2,3,1:T(8,128)(2,1)S(1)} %bitcast.74, bf16[128,2,2,128]{3,0,2,1:T(8,128)(2,1)} %get-tuple-element.344), kind=kOutput, calls=%fused_computation.19.clone.1 | convolution fusion | flops 17497600 | bytes 739344 | tf_op jit(solution)/shard_map/while/body/eval_jaxpr/qgrd,sgd->grqs/dot_general | solution.py:23
  44.3 5.4 %reduce_window_sum.34 = f32[2,2,128,128]{2,3,1,0:T(8,128)S(1)} reduce-window(f32[2,2,128,128]{2,3,1,0:T(8,128)} %get-tuple-element.307, f32[]{:T(128)} %constant.57.clone.1..sunk), window={size=1x1x1x128 pad=0_0x0_0x0_0x0_127}, to_apply=%region_3.3 | reduce-window | flops 8323072 | bytes 524292 | tf_op jit(solution)/shard_map/while/body/eval_jaxpr/reduce_window_sum | solution.py:33
  56.4 2.6 %collective-permute-start.2 = (bf16[128,256]{0,1:T(8,128)(2,1)}, bf16[128,256]{0,1:T(8,128)(2,1)S(1)}, u32[]{:S(2)}, u32[]{:S(2)}) collective-permute-start(bf16[128,256]{0,1:T(8,128)(2,1)} %get-tuple-element.326), channel_id=1, source_target_pairs={{0,4},{4,8},{8,12},{1,5},{5,9},{9,13},{2,6},{6,10},{10,14},{3,7},{... | collective-permute-start | bytes 196616 | tf_op jit(solution)/shard_map/while/body/eval_jaxpr/ppermute | solution.py:16
  63.0 2.6 %fusion.80 = (f32[2,2,128]{2,1,0:T(2,128)}, f32[2,2,128,128]{2,3,1,0:T(8,128)}, f32[2,2,128,128]{2,3,1,0:T(8,128)}) fusion(pred[128,128]{0,1:T(8,128)(4,1)S(1)} %compare_and_fusion.2, f32[2,2]{1,0:T(2,128)S(1)} %add.252, bf16[128,2,128,1]{0,2,3,1:T(8,128)(2,1)S(1)} %bitcast.74, bf16[128,2,2,128]{3,0,2,1:T(8,128)(2,1)} %get-tuple-element.344), kind=kOutput, calls=%fused_computation.19.clone.1 | convolution fusion | flops 17497600 | bytes 739344 | tf_op jit(solution)/shard_map/while/body/eval_jaxpr/qgrd,sgd->grqs/dot_general | solution.py:23
  65.6 5.4 %reduce_window_sum.34 = f32[2,2,128,128]{2,3,1,0:T(8,128)S(1)} reduce-window(f32[2,2,128,128]{2,3,1,0:T(8,128)} %get-tuple-element.307, f32[]{:T(128)} %constant.57.clone.1..sunk), window={size=1x1x1x128 pad=0_0x0_0x0_0x0_127}, to_apply=%region_3.3 | reduce-window | flops 8323072 | bytes 524292 | tf_op jit(solution)/shard_map/while/body/eval_jaxpr/reduce_window_sum | solution.py:33
  75.8 2.7 %collective-permute-start.1 = (bf16[128,1]{0,1:T(2,128)(2,1)}, bf16[128,1]{0,1:T(2,128)(2,1)S(1)}, u32[]{:S(2)}, u32[]{:S(2)}) collective-permute-start(bf16[128,1]{0,1:T(2,128)(2,1)} %get-tuple-element.328), channel_id=1, source_target_pairs={{0,4},{4,8},{8,12},{1,5},{5,9},{9,13},{2,6},{6,10},{10,14},{3,7},{... | collective-permute-start | bytes 776 | tf_op jit(solution)/shard_map/while/body/eval_jaxpr/ppermute | solution.py:16
  84.7 2.6 %fusion.80 = (f32[2,2,128]{2,1,0:T(2,128)}, f32[2,2,128,128]{2,3,1,0:T(8,128)}, f32[2,2,128,128]{2,3,1,0:T(8,128)}) fusion(pred[128,128]{0,1:T(8,128)(4,1)S(1)} %compare_and_fusion.2, f32[2,2]{1,0:T(2,128)S(1)} %add.252, bf16[128,2,128,1]{0,2,3,1:T(8,128)(2,1)S(1)} %bitcast.74, bf16[128,2,2,128]{3,0,2,1:T(8,128)(2,1)} %get-tuple-element.344), kind=kOutput, calls=%fused_computation.19.clone.1 | convolution fusion | flops 17497600 | bytes 739344 | tf_op jit(solution)/shard_map/while/body/eval_jaxpr/qgrd,sgd->grqs/dot_general | solution.py:23
  87.3 5.4 %reduce_window_sum.34 = f32[2,2,128,128]{2,3,1,0:T(8,128)S(1)} reduce-window(f32[2,2,128,128]{2,3,1,0:T(8,128)} %get-tuple-element.307, f32[]{:T(128)} %constant.57.clone.1..sunk), window={size=1x1x1x128 pad=0_0x0_0x0_0x0_127}, to_apply=%region_3.3 | reduce-window | flops 8323072 | bytes 524292 | tf_op jit(solution)/shard_map/while/body/eval_jaxpr/reduce_window_sum | solution.py:33
  92.7 2.3 fusion.81
  98.6 2.9 %convolution_convert_fusion.1 = bf16[128,2048]{1,0:T(8,128)(2,1)} fusion(bf16[128,512]{0,1:T(8,128)(2,1)S(1)} %bitcast.79, bf16[512,2048]{1,0:T(8,128)(2,1)} %param.20), kind=kOutput, calls=%fused_computation.28 | convolution fusion | flops 268697600 | bytes 2752512 | tf_op jit(solution)/shard_map/dot_general | solution.py:92
  102.6 19.0 %reduce-scatter.3.cloned.1.call-done = bf16[32,2048]{1,0:T(8,128)(2,1)} async-done(((bf16[128,2048]{1,0:T(8,128)(2,1)}), bf16[32,2048]{1,0:T(8,128)(2,1)}) %reduce-scatter.3.cloned.1.call-update) | async-done | bytes 131088 | tf_op jit(solution)/shard_map/reduce_scatter | solution.py:91
  123.9 18.8 %all_to_all.10 = bf16[4,32,2048]{2,1,0:T(8,128)(2,1)} all-to-all(bf16[4,32,2048]{2,1,0:T(8,128)(2,1)S(1)} %bitcast.73), channel_id=1, replica_groups=mesh['grp'=2,'sp'=4,'tp'=4] {'sp'}, dimensions={0} | all-to-all | bytes 1048576 | tf_op jit(solution)/shard_map/all_to_all | solution.py:120
  142.8 20.8 %all-gather.2.cloned.1.call-done = bf16[16,32,2048]{2,1,0:T(8,128)(2,1)} async-done(((bf16[4,32,2048]{2,1,0:T(8,128)(2,1)}), bf16[16,32,2048]{2,1,0:T(8,128)(2,1)}) %all-gather.2.cloned.1.call-update) | async-done | bytes 2097168 | tf_op jit(solution)/shard_map/all_gather | solution.py:121
  163.6 4.5 %fusion.21 = f32[512,768]{1,0:T(8,128)S(1)} fusion(bf16[512,2048]{1,0:T(8,128)(2,1)} %bitcast.83, bf16[1,2048,768]{2,1,0:T(8,128)(2,1)} %param.25), kind=kOutput, calls=%fused_computation.24 | convolution fusion | flops 1610612736 | bytes 6815744 | tf_op jit(solution)/shard_map/dot_general | solution.py:123
  170.0 3.2 %fusion.23 = bf16[4,128,2048]{2,1,0:T(8,128)(2,1)} fusion(bf16[4,128,768]{2,1,0:T(8,128)(2,1)S(1)} %bitcast.85, bf16[1,768,2048]{2,1,0:T(8,128)(2,1)S(1)} %copy-done), kind=kOutput, calls=%fused_computation.26 | convolution fusion | flops 1611661312 | bytes 6029312 | tf_op jit(solution)/shard_map/dot_general | solution.py:126
  173.3 31.3 %reduce-scatter.5.cloned.1.call-done = bf16[1,128,2048]{2,1,0:T(8,128)(2,1)} async-done(((bf16[4,128,2048]{2,1,0:T(8,128)(2,1)}), bf16[1,128,2048]{2,1,0:T(8,128)(2,1)}) %reduce-scatter.5.cloned.1.call-update) | async-done | bytes 524304 | tf_op jit(solution)/shard_map/reduce_scatter | solution.py:127
  204.6 4.6 %all-to-all-start.1 = ((bf16[4,32,2048]{2,1,0:T(8,128)(2,1)}), bf16[4,32,2048]{2,1,0:T(8,128)(2,1)}, u32[]{:S(2)}, u32[]{:S(2)}) async-start(bf16[4,32,2048]{2,1,0:T(8,128)(2,1)} %bitcast.76), calls=%async_computation.3 | async-start | bytes 1048576 | tf_op jit(solution)/shard_map/all_to_all | solution.py:134
  209.3 14.3 %all-to-all-done.1 = bf16[4,32,2048]{2,1,0:T(8,128)(2,1)} async-done(((bf16[4,32,2048]{2,1,0:T(8,128)(2,1)}), bf16[4,32,2048]{2,1,0:T(8,128)(2,1)}, u32[]{:S(2)}, u32[]{:S(2)}) %all-to-all-start.1) | async-done | bytes 524320 | tf_op jit(solution)/shard_map/all_to_all | solution.py:134
  (84 shorter events, 48.3 us)
Async XLA Ops:
  6.5 163.5 %copy-start = (bf16[1,768,2048]{2,1,0:T(8,128)(2,1)S(1)}, bf16[1,768,2048]{2,1,0:T(8,128)(2,1)}, u32[]{:S(2)}) copy-start(bf16[1,768,2048]{2,1,0:T(8,128)(2,1)} %param.27) | copy-start | bytes 9437188
  6.5 115.0 %reduce-scatter.3.cloned.1.call-start = ((), (), s32[]{:S(2)}) async-start(), calls=%async_computation.4 | async-start | bytes 655360 | tf_op jit(solution)/shard_map/reduce_scatter | solution.py:91
  27.7 12.7 %collective-permute-start.1 = (bf16[128,1]{0,1:T(2,128)(2,1)}, bf16[128,1]{0,1:T(2,128)(2,1)S(1)}, u32[]{:S(2)}, u32[]{:S(2)}) collective-permute-start(bf16[128,1]{0,1:T(2,128)(2,1)} %get-tuple-element.328), channel_id=1, source_target_pairs={{0,4},{4,8},{8,12},{1,5},{5,9},{9,13},{2,6},{6,10},{10,14},{3,7},{... | collective-permute-start | bytes 776 | tf_op jit(solution)/shard_map/while/body/eval_jaxpr/ppermute | solution.py:16
  32.7 9.0 %collective-permute-start.2 = (bf16[128,256]{0,1:T(8,128)(2,1)}, bf16[128,256]{0,1:T(8,128)(2,1)S(1)}, u32[]{:S(2)}, u32[]{:S(2)}) collective-permute-start(bf16[128,256]{0,1:T(8,128)(2,1)} %get-tuple-element.326), channel_id=1, source_target_pairs={{0,4},{4,8},{8,12},{1,5},{5,9},{9,13},{2,6},{6,10},{10,14},{3,7},{... | collective-permute-start | bytes 196616 | tf_op jit(solution)/shard_map/while/body/eval_jaxpr/ppermute | solution.py:16
  36.2 13.5 %collective-permute-start = (bf16[128,256]{0,1:T(8,128)(2,1)}, bf16[128,256]{0,1:T(8,128)(2,1)S(1)}, u32[]{:S(2)}, u32[]{:S(2)}) collective-permute-start(bf16[128,256]{0,1:T(8,128)(2,1)} %get-tuple-element.327), channel_id=1, source_target_pairs={{0,4},{4,8},{8,12},{1,5},{5,9},{9,13},{2,6},{6,10},{10,14},{3,7},{... | collective-permute-start | bytes 196616 | tf_op jit(solution)/shard_map/while/body/eval_jaxpr/ppermute | solution.py:16
  54.5 7.2 %collective-permute-start.1 = (bf16[128,1]{0,1:T(2,128)(2,1)}, bf16[128,1]{0,1:T(2,128)(2,1)S(1)}, u32[]{:S(2)}, u32[]{:S(2)}) collective-permute-start(bf16[128,1]{0,1:T(2,128)(2,1)} %get-tuple-element.328), channel_id=1, source_target_pairs={{0,4},{4,8},{8,12},{1,5},{5,9},{9,13},{2,6},{6,10},{10,14},{3,7},{... | collective-permute-start | bytes 776 | tf_op jit(solution)/shard_map/while/body/eval_jaxpr/ppermute | solution.py:16
  56.4 6.6 %collective-permute-start.2 = (bf16[128,256]{0,1:T(8,128)(2,1)}, bf16[128,256]{0,1:T(8,128)(2,1)S(1)}, u32[]{:S(2)}, u32[]{:S(2)}) collective-permute-start(bf16[128,256]{0,1:T(8,128)(2,1)} %get-tuple-element.326), channel_id=1, source_target_pairs={{0,4},{4,8},{8,12},{1,5},{5,9},{9,13},{2,6},{6,10},{10,14},{3,7},{... | collective-permute-start | bytes 196616 | tf_op jit(solution)/shard_map/while/body/eval_jaxpr/ppermute | solution.py:16
  59.0 12.0 %collective-permute-start = (bf16[128,256]{0,1:T(8,128)(2,1)}, bf16[128,256]{0,1:T(8,128)(2,1)S(1)}, u32[]{:S(2)}, u32[]{:S(2)}) collective-permute-start(bf16[128,256]{0,1:T(8,128)(2,1)} %get-tuple-element.327), channel_id=1, source_target_pairs={{0,4},{4,8},{8,12},{1,5},{5,9},{9,13},{2,6},{6,10},{10,14},{3,7},{... | collective-permute-start | bytes 196616 | tf_op jit(solution)/shard_map/while/body/eval_jaxpr/ppermute | solution.py:16
  75.8 7.6 %collective-permute-start.1 = (bf16[128,1]{0,1:T(2,128)(2,1)}, bf16[128,1]{0,1:T(2,128)(2,1)S(1)}, u32[]{:S(2)}, u32[]{:S(2)}) collective-permute-start(bf16[128,1]{0,1:T(2,128)(2,1)} %get-tuple-element.328), channel_id=1, source_target_pairs={{0,4},{4,8},{8,12},{1,5},{5,9},{9,13},{2,6},{6,10},{10,14},{3,7},{... | collective-permute-start | bytes 776 | tf_op jit(solution)/shard_map/while/body/eval_jaxpr/ppermute | solution.py:16
  78.5 6.2 %collective-permute-start.2 = (bf16[128,256]{0,1:T(8,128)(2,1)}, bf16[128,256]{0,1:T(8,128)(2,1)S(1)}, u32[]{:S(2)}, u32[]{:S(2)}) collective-permute-start(bf16[128,256]{0,1:T(8,128)(2,1)} %get-tuple-element.326), channel_id=1, source_target_pairs={{0,4},{4,8},{8,12},{1,5},{5,9},{9,13},{2,6},{6,10},{10,14},{3,7},{... | collective-permute-start | bytes 196616 | tf_op jit(solution)/shard_map/while/body/eval_jaxpr/ppermute | solution.py:16
  80.7 12.0 %collective-permute-start = (bf16[128,256]{0,1:T(8,128)(2,1)}, bf16[128,256]{0,1:T(8,128)(2,1)S(1)}, u32[]{:S(2)}, u32[]{:S(2)}) collective-permute-start(bf16[128,256]{0,1:T(8,128)(2,1)} %get-tuple-element.327), channel_id=1, source_target_pairs={{0,4},{4,8},{8,12},{1,5},{5,9},{9,13},{2,6},{6,10},{10,14},{3,7},{... | collective-permute-start | bytes 196616 | tf_op jit(solution)/shard_map/while/body/eval_jaxpr/ppermute | solution.py:16
  97.5 4.2 %copy-start.4 = (s32[32,2]{0,1:T(2,128)S(1)}, s32[32,2]{0,1:T(2,128)}, u32[]{:S(2)}) copy-start(s32[32,2]{0,1:T(2,128)} %param.23) | copy-start | bytes 772
  97.5 24.1 %copy-start.1 = (bf16[32,2048]{1,0:T(8,128)(2,1)S(1)}, bf16[32,2048]{1,0:T(8,128)(2,1)}, u32[]{:S(2)}) copy-start(bf16[32,2048]{1,0:T(8,128)(2,1)} %param.21) | copy-start | bytes 393220
  97.5 25.1 %copy-start.3 = (f32[2048]{0:T(1024)S(1)}, f32[2048]{0:T(1024)}, u32[]{:S(2)}) copy-start(f32[2048]{0:T(1024)} %param.22) | copy-start | bytes 24580
  101.5 62.1 %all-gather.2.cloned.1.call-start = ((), (), s32[]{:S(2)}) async-start(), calls=%async_computation.5 | async-start | bytes 2621440 | tf_op jit(solution)/shard_map/all_gather | solution.py:121
  142.8 61.8 %reduce-scatter.5.cloned.1.call-start = ((), (), s32[]{:S(2)}) async-start(), calls=%async_computation.6 | async-start | bytes 2621440 | tf_op jit(solution)/shard_map/reduce_scatter | solution.py:127
  163.6 4.5 %copy-start.6 = (bf16[1,2048,768]{2,1,0:T(8,128)(2,1)S(1)}, bf16[1,2048,768]{2,1,0:T(8,128)(2,1)}, u32[]{:S(2)}) copy-start(bf16[1,2048,768]{2,1,0:T(8,128)(2,1)} %param.26) | copy-start | bytes 9437188
  163.6 4.5 %copy-start.7 = (bf16[16,32,2048]{2,1,0:T(8,128)(2,1)S(1)}, bf16[16,32,2048]{2,1,0:T(8,128)(2,1)}, u32[]{:S(2)}) copy-start(bf16[16,32,2048]{2,1,0:T(8,128)(2,1)} %all-gather.2.cloned.1.call-done) | copy-start | bytes 6291460
  173.2 50.4 %copy-start.5 = (f32[32,2]{0,1:T(2,128)S(1)}, f32[32,2]{0,1:T(2,128)}, u32[]{:S(2)}) copy-start(f32[32,2]{0,1:T(2,128)} %param.24) | copy-start | bytes 772
  173.2 51.7 %copy-start.2 = (bf16[32,2048]{1,0:T(8,128)(2,1)S(1)}, bf16[32,2048]{1,0:T(8,128)(2,1)}, u32[]{:S(2)}) copy-start(bf16[32,2048]{1,0:T(8,128)(2,1)} %reduce-scatter.3.cloned.1.call-done) | copy-start | bytes 393220
  204.6 19.1 %all-to-all-start.1 = ((bf16[4,32,2048]{2,1,0:T(8,128)(2,1)}), bf16[4,32,2048]{2,1,0:T(8,128)(2,1)}, u32[]{:S(2)}, u32[]{:S(2)}) async-start(bf16[4,32,2048]{2,1,0:T(8,128)(2,1)} %bitcast.76), calls=%async_computation.3 | async-start | bytes 1048576 | tf_op jit(solution)/shard_map/all_to_all | solution.py:134
Sparse Core Ops, SparseCore 0:
  101.7 19.8 reduce-scatter.2
  142.9 20.6 all-gather.1
  173.4 31.1 reduce-scatter.4
where the time goes:
time: 233 us; the launch traced here: 232 us
  waiting for transfers between devices  85.5 us (37%)
  matrix products  34.5 us (15%)
  other arithmetic  31.5 us (14%)
  starting transfers between devices  30.1 us (13%)
  blocking collectives  18.8 us (8%)
  local copies, waits for them, and re-layouts  18.3 us (8%)
  between operations  13.2 us (6%)
    reduce_scatter x1, waiting for transfers between devices, local(): lax.psum_scatter(partial_out.reshape(tp_count, sp_count * slot_limit, D)....  31.3 us
    ppermute x9, starting transfers between devices, passed_along(): lax.ppermute(value, axis, [(source, source + steps) for source in range(i...  25.2 us
    another operation x4, other arithmetic, attend_terms(): lax.cumsum(keep, axis=3, reverse=True) - keep + carried[:, :, :, None]  21.2 us
    all_gather x1, waiting for transfers between devices, local(): gathered = lax.all_gather(arrived, 'tp', axis=0, tiled=True)  20.8 us
    reduce_scatter x1, waiting for transfers between devices, local(): lax.psum_scatter(jnp.dot(mixed, w_out, preferred_element_type=jnp.float32...  19 us
    all_to_all x1, blocking collectives, local(): lax.all_to_all(outgoing, 'sp', split_axis=0, concat_axis=0, tiled=True)  18.8 us
    all_to_all x1, waiting for transfers between devices, local(): lax.all_to_all(expert_result, 'sp', split_axis=0, concat_axis=0, tiled=True)  14.3 us
    dot_general x4, matrix products, attend_terms(): jnp.einsum('qgrd,sgd->grqs', query_grid, key_block.reshape(key_count, kv_...  10.4 us
  transfers between devices with their start and end apart: 13, of which 4 were waited for; matrix products, arithmetic and copies ran while one was open for 13% of the time, Pallas kernels for 0%

commit v1 on v0

--- a/solution.py
+++ b/solution.py
@@ -1,6 +1,10 @@
+import functools
+
 import jax
 import jax.numpy as jnp
 from jax import lax
+from jax.experimental import pallas as pl
+from jax.experimental.pallas import tpu as pltpu
 from jax.sharding import PartitionSpec as P
 
 D = 2048
@@ -137,9 +141,501 @@
     return (middle_value + combined).astype(jnp.bfloat16)
 
 
+MESH = pl.DeviceIdType.MESH
+
+
+def paired(index, turn, count):
+    result, bit = 0, 1
+    while bit < count:
+        a, b = lax.rem(index // bit, 2), lax.rem(turn // bit, 2)
+        result = result + bit * (a + b - 2 * a * b)
+        bit *= 2
+    return result
+
+
+def fused_kernel(
+    sp_count,
+    tp_count,
+    q_ref,
+    k_ref,
+    v_ref,
+    bias_ref,
+    doc_ref,
+    resid_ref,
+    gain_ref,
+    ids_ref,
+    gates_ref,
+    w_out_hbm,
+    w_gate_hbm,
+    w_up_hbm,
+    w_down_hbm,
+    out_ref,
+    w_out,
+    w_gate,
+    w_up,
+    w_down,
+    k_all,
+    v_all,
+    doc_all,
+    mix_acc,
+    carry,
+    mixed,
+    middle,
+    x_all,
+    hidden,
+    part,
+    sib_in,
+    x_out,
+    x_in,
+    z_out,
+    returned,
+    w_sem,
+    kv_send,
+    kv_recv,
+    z_send,
+    z_recv,
+    gx_send,
+    gx_recv,
+    gs_send,
+    gs_recv,
+    ps_send,
+    ps_recv,
+    px_send,
+    px_recv,
+    rz_send,
+    rz_recv,
+):
+    s = lax.axis_index("sp")
+    t = lax.axis_index("tp")
+    width = tp_count // 2
+    x, c = t // 2, lax.rem(t, 2)
+    sibling = 2 * x + 1 - c
+    tok = q_ref.shape[0]
+    kv_local = k_ref.shape[1] // DH
+    rep = q_ref.shape[1] // k_ref.shape[1]
+    rows, model = resid_ref.shape
+    ff = w_up.shape[1]
+    f32, bf16 = jnp.float32, jnp.bfloat16
+
+    loads = [
+        pltpu.make_async_copy(src, dst, w_sem.at[j])
+        for j, (src, dst) in enumerate(
+            (
+                (w_out_hbm, w_out),
+                (w_gate_hbm.at[0], w_gate),
+                (w_up_hbm.at[0], w_up),
+                (w_down_hbm.at[0], w_down),
+            )
+        )
+    ]
+    for load in loads:
+        load.start()
+
+    barrier = pltpu.get_barrier_semaphore()
+    for j in range(1, sp_count):
+        pl.semaphore_signal(
+            barrier, inc=1, device_id={"sp": lax.rem(s + j, sp_count)}, device_id_type=MESH
+        )
+    for j in range(1, tp_count):
+        pl.semaphore_signal(
+            barrier, inc=1, device_id={"tp": lax.rem(t + j, tp_count)}, device_id_type=MESH
+        )
+    pl.semaphore_wait(barrier, sp_count + tp_count - 2)
+
+    def remote(src, dst, send, recv, device):
+        return pltpu.make_async_remote_copy(
+            src_ref=src,
+            dst_ref=dst,
+            send_sem=send,
+            recv_sem=recv,
+            device_id=device,
+            device_id_type=MESH,
+        )
+
+    def passed(hop):
+        right = {"sp": lax.rem(s + 1, sp_count)}
+        own = (k_ref, v_ref, doc_ref)
+        slots = (k_all, v_all, doc_all)
+        return [
+            remote(
+                own[j] if hop == 0 else slots[j].at[hop - 1],
+                slots[j].at[hop],
+                kv_send.at[hop, j],
+                kv_recv.at[hop, j],
+                right,
+            )
+            for j in range(3)
+        ]
+
+    has_right = s < sp_count - 1
+
+    @pl.when(has_right)
+    def _():
+        for copy in passed(0):
+            copy.start()
+
+    at_row = lax.broadcasted_iota(jnp.int32, (tok, tok), 0)
+    at_col = lax.broadcasted_iota(jnp.int32, (tok, tok), 1)
+    summing = jnp.concatenate(
+        [(at_row > at_col).astype(f32), jnp.ones((tok, tok), f32)], axis=1
+    ).astype(bf16)
+    doc_query = jnp.broadcast_to(doc_ref[...].astype(f32), (tok, tok)).T
+
+    def attend(hop):
+        docs = doc_ref[...] if hop == 0 else doc_all[hop - 1]
+        live = doc_query == jnp.broadcast_to(docs.astype(f32), (tok, tok))
+        if hop == 0:
+            live = live & (at_col < at_row)
+        live_f = jnp.concatenate([live.astype(f32)] * rep, axis=0)
+        live_all = live_f > 0.5
+        for g in range(kv_local):
+            heads = [g * rep + r for r in range(rep)]
+            query = jnp.concatenate([q_ref[:, h * DH : (h + 1) * DH] for h in heads], axis=0)
+            bias = jnp.concatenate([jnp.full((tok, tok), bias_ref[h], f32) for h in heads], axis=0)
+            lanes = slice(g * DH, (g + 1) * DH)
+            key = k_ref[:, lanes] if hop == 0 else k_all[hop - 1, :, lanes]
+            value = v_ref[:, lanes] if hop == 0 else v_all[hop - 1, :, lanes]
+            logits = (
+                lax.dot_general(
+                    query, key, (((1,), (1,)), ((), ())), preferred_element_type=f32
+                )
+                * DH ** (-0.5)
+                + bias
+            )
+            keep_any = -(jnp.maximum(logits, 0.0) + jnp.log1p(jnp.exp(-jnp.abs(logits))))
+            keep = jnp.where(live_all, keep_any, 0.0)
+            high = keep.astype(bf16)
+            rest = keep - high.astype(f32)
+            mid = rest.astype(bf16)
+            low = (rest - mid.astype(f32)).astype(bf16)
+            sums = (
+                jnp.dot(high, summing, preferred_element_type=f32)
+                + jnp.dot(mid, summing, preferred_element_type=f32)
+                + jnp.dot(low, summing, preferred_element_type=f32)
+            )
+            after, total = sums[:, :tok], sums[:, tok:]
+            if hop > 0:
+                after = after + carry[g]
+                total = total + carry[g]
+            carry[g] = total
+            weight = jnp.where(live_all, jnp.exp(logits + keep_any + after), 0.0).astype(bf16)
+            mix = jnp.dot(weight, value, preferred_element_type=f32)
+            mix_acc[g] = mix if hop == 0 else mix_acc[g] + mix
+
+    attend(0)
+    for hop in range(1, sp_count):
+
+        @pl.when(s >= hop)
+        def _():
+            for copy in passed(hop - 1):
+                copy.wait_recv()
+            if hop < sp_count - 1:
+
+                @pl.when(has_right)
+                def _():
+                    for copy in passed(hop):
+                        copy.start()
+
+            attend(hop)
+
+    for g in range(kv_local):
+        for r in range(rep):
+            h = g * rep + r
+            mixed[:, h * DH : (h + 1) * DH] = mix_acc[g, r * tok : (r + 1) * tok, :].astype(bf16)
+
+    def pair_copies(i):
+        return [
+            remote(
+                part.at[i, 2 * j + 1 - c],
+                sib_in.at[i, j],
+                ps_send.at[i, j],
+                ps_recv.at[i, j],
+                {"tp": sibling},
+            )
+            for j in range(width)
+        ]
+
+    def across_copies(i):
+        return [
+            remote(
+                x_out.at[i, j - 1],
+                x_in.at[i, j - 1],
+                px_send.at[i, j - 1],
+                px_recv.at[i, j - 1],
+                {"tp": 2 * lax.rem(x + j, width) + c},
+            )
+            for j in range(1, width)
+        ]
+
+    def pair_sum(i, at):
+        return part[i, 2 * at + c].astype(f32) + sib_in[i, at].astype(f32)
+
+    def sum_pairs(i):
+        for copy in pair_copies(i):
+            copy.wait_recv()
+        for j, copy in enumerate(across_copies(i)):
+            x_out[i, j] = pair_sum(i, lax.rem(x + j + 1, width)).astype(bf16)
+            copy.start()
+
+    def sum_across(i):
+        result = pair_sum(i, x)
+        for j, copy in enumerate(across_copies(i)):
+            copy.wait_recv()
+            result = result + x_in[i, j].astype(f32)
+        return result
+
+    loads[0].wait()
+    step = 512 if model % 512 == 0 else model
+
+    def project(n, _):
+        columns = pl.ds(pl.multiple_of(n * step, step), step)
+        value = jnp.dot(mixed[...], w_out[:, columns], preferred_element_type=f32)
+        part[sp_count, :, :, columns] = value.astype(bf16).reshape(tp_count, rows, step)
+        return 0
+
+    lax.fori_loop(0, model // step, project, 0)
+    for copy in pair_copies(sp_count):
+        copy.start()
+    sum_pairs(sp_count)
+    mid_value = (resid_ref[...].astype(f32) + sum_across(sp_count)).astype(bf16).astype(f32)
+    middle[...] = mid_value
+    x_all[s, t] = (
+        mid_value
+        * lax.rsqrt(jnp.mean(mid_value * mid_value, axis=1, keepdims=True) + 1e-06)
+        * gain_ref[...]
+    ).astype(bf16)
+
+    def along_copy(i):
+        return remote(
+            x_all.at[s, t],
+            x_all.at[s, t],
+            z_send.at[i],
+            z_recv.at[i],
+            {"sp": paired(s, i, sp_count)},
+        )
+
+    def spread_copies(i):
+        block = x_all.at[paired(s, i, sp_count), t]
+        return [
+            remote(
+                block,
+                block,
+                gx_send.at[i, j - 1],
+                gx_recv.at[i, j - 1],
+                {"tp": 2 * lax.rem(x + j, width) + c},
+            )
+            for j in range(1, width)
+        ]
+
+    def twin_copy(i, j):
+        block = x_all.at[paired(s, i, sp_count), 2 * lax.rem(x - j + width, width) + c]
+        return remote(block, block, gs_send.at[i, j], gs_recv.at[i, j], {"tp": sibling})
+
+    def spread(i):
+        for copy in spread_copies(i):
+            copy.start()
+        twin_copy(i, 0).start()
+
+    def return_copy(i):
+        return remote(
+            z_out.at[i],
+            returned.at[i],
+            rz_send.at[i],
+            rz_recv.at[i],
+            {"sp": paired(s, i, sp_count)},
+        )
+
+    spread(0)
+    for i in range(1, sp_count):
+        along_copy(i).start()
+    for load in loads[1:]:
+        load.wait()
+
+    f_step = 256 if ff % 256 == 0 else ff
+
+    def turn(i, _):
+        @pl.when(i + 1 < sp_count)
+        def _():
+            along_copy(i + 1).wait_recv()
+            spread(i + 1)
+
+        @pl.when(i < sp_count)
+        def _():
+            for j, copy in enumerate(spread_copies(i)):
+                copy.wait_recv()
+                twin_copy(i, j + 1).start()
+            for j in range(width):
+                twin_copy(i, j).wait_recv()
+            rows_in = x_all[paired(s, i, sp_count)].reshape(tp_count * rows, model)
+
+            def widen(n, _):
+                columns = pl.ds(pl.multiple_of(n * f_step, f_step), f_step)
+                gate = jnp.dot(rows_in, w_gate[:, columns], preferred_element_type=f32)
+                up = jnp.dot(rows_in, w_up[:, columns], preferred_element_type=f32)
+                hidden[:, columns] = (gate / (1.0 + jnp.exp(-gate)) * up).astype(bf16)
+                return 0
+
+            lax.fori_loop(0, ff // f_step, widen, 0)
+
+            def narrow(n, _):
+                columns = pl.ds(pl.multiple_of(n * step, step), step)
+                value = jnp.dot(hidden[...], w_down[:, columns], preferred_element_type=f32)
+                part[i, :, :, columns] = value.astype(bf16).reshape(tp_count, rows, step)
+                return 0
+
+            lax.fori_loop(0, model // step, narrow, 0)
+            for copy in pair_copies(i):
+                copy.start()
+
+        @pl.when((i >= 1) & (i <= sp_count))
+        def _():
+            sum_pairs(i - 1)
+
+        @pl.when(i >= 2)
+        def _():
+            z_out[i - 2] = sum_across(i - 2).astype(bf16)
+
+            @pl.when(i > 2)
+            def _():
+                return_copy(i - 2).start()
+
+        return 0
+
+    lax.fori_loop(0, sp_count + 2, turn, 0)
+
+    result = middle[...]
+    for i in range(sp_count):
+        if i > 0:
+            return_copy(i).wait_recv()
+        chosen = ids_ref[...] == paired(s, i, sp_count)
+        gate = jnp.sum(jnp.where(chosen, gates_ref[...], 0.0), axis=1, keepdims=True)
+        value = z_out[0] if i == 0 else returned[i]
+        result = result + gate * value.astype(f32)
+    out_ref[...] = result.astype(bf16)
+
+    for hop in range(sp_count - 1):
+
+        @pl.when(has_right & (s >= hop))
+        def _():
+            for copy in passed(hop):
+                copy.wait_send()
+
+    for i in range(sp_count + 1):
+        for copy in pair_copies(i) + across_copies(i):
+            copy.wait_send()
+    for i in range(sp_count):
+        if i > 0:
+            along_copy(i).wait_send()
+            return_copy(i).wait_send()
+        for copy in spread_copies(i):
+            copy.wait_send()
+        for j in range(width):
+            twin_copy(i, j).wait_send()
+
+
+def fused(
+    queries,
+    keys,
+    values,
+    head_bias,
+    documents,
+    w_out,
+    resid,
+    norm_gain,
+    expert_ids,
+    expert_gates,
+    w_gate,
+    w_up,
+    w_down,
+):
+    sp_count, tp_count = lax.axis_size("sp"), lax.axis_size("tp")
+    width = tp_count // 2
+    tok = queries.shape[0]
+    kv_local = keys.shape[1] // DH
+    rep = queries.shape[1] // keys.shape[1]
+    rows, model = resid.shape
+    ff = w_up.shape[2]
+    bf16, f32 = jnp.bfloat16, jnp.float32
+    dma = pltpu.SemaphoreType.DMA
+    vmem, hbm = pl.BlockSpec(memory_space=pltpu.VMEM), pl.BlockSpec(memory_space=pl.ANY)
+    return pl.pallas_call(
+        functools.partial(fused_kernel, sp_count, tp_count),
+        out_shape=jax.ShapeDtypeStruct((rows, model), bf16),
+        in_specs=[vmem] * 3
+        + [pl.BlockSpec(memory_space=pltpu.SMEM)]
+        + [vmem] * 5
+        + [hbm] * 4,
+        out_specs=vmem,
+        scratch_shapes=[
+            pltpu.VMEM(w_out.shape, bf16),
+            pltpu.VMEM(w_gate.shape[1:], bf16),
+            pltpu.VMEM(w_up.shape[1:], bf16),
+            pltpu.VMEM(w_down.shape[1:], bf16),
+            pltpu.VMEM((sp_count - 1,) + keys.shape, bf16),
+            pltpu.VMEM((sp_count - 1,) + values.shape, bf16),
+            pltpu.VMEM((sp_count - 1, 1, tok), jnp.int32),
+            pltpu.VMEM((kv_local, rep * tok, DH), f32),
+            pltpu.VMEM((kv_local, rep * tok, tok), f32),
+            pltpu.VMEM(queries.shape, bf16),
+            pltpu.VMEM((rows, model), f32),
+            pltpu.VMEM((sp_count, tp_count, rows, model), bf16),
+            pltpu.VMEM((tp_count * rows, ff), bf16),
+            pltpu.VMEM((sp_count + 1, tp_count, rows, model), bf16),
+            pltpu.VMEM((sp_count + 1, width, rows, model), bf16),
+            pltpu.VMEM((sp_count + 1, width - 1, rows, model), bf16),
+            pltpu.VMEM((sp_count + 1, width - 1, rows, model), bf16),
+            pltpu.VMEM((sp_count, rows, model), bf16),
+            pltpu.VMEM((sp_count, rows, model), bf16),
+            dma((4,)),
+            dma((sp_count - 1, 3)),
+            dma((sp_count - 1, 3)),
+            dma((sp_count,)),
+            dma((sp_count,)),
+            dma((sp_count, width - 1)),
+            dma((sp_count, width - 1)),
+            dma((sp_count, width)),
+            dma((sp_count, width)),
+            dma((sp_count + 1, width)),
+            dma((sp_count + 1, width)),
+            dma((sp_count + 1, width - 1)),
+            dma((sp_count + 1, width - 1)),
+            dma((sp_count,)),
+            dma((sp_count,)),
+        ],
+        compiler_params=pltpu.CompilerParams(
+            collective_id=0, has_side_effects=True, vmem_limit_bytes=60 * 2**20
+        ),
+    )(
+        queries,
+        keys,
+        values,
+        head_bias,
+        documents.reshape(1, tok),
+        resid,
+        norm_gain.reshape(1, model),
+        expert_ids,
+        expert_gates,
+        w_out,
+        w_gate,
+        w_up,
+        w_down,
+    )
+
+
+def block(*arrays):
+    queries, resid, w_gate = arrays[0], arrays[6], arrays[10]
+    sp_count, tp_count = lax.axis_size("sp"), lax.axis_size("tp")
+    rows = resid.shape[0]
+    slots = min(rows, max(2, 2 * TOPK * rows // (w_gate.shape[0] * sp_count)))
+    powers = sp_count & (sp_count - 1) == 0 and tp_count % 2 == 0 and min(sp_count, tp_count // 2) > 1
+    if slots == rows and w_gate.shape[0] == 1 and powers and queries.shape[0] == DH:
+        return fused(*arrays)
+    return local(*arrays)
+
+
 def solution(mesh):
     return jax.shard_map(
-        local,
+        block,
         mesh=mesh,
         in_specs=(
             P(("grp", "sp"), "tp"),

time: 233 us -> 73.4 us (0.32)
  waiting for transfers between devices: 85.5 us -> 0 us
  Pallas kernels: 0 us -> 68.5 us
  matrix products: 34.5 us -> 0 us
  other arithmetic: 31.5 us -> 0 us
  starting transfers between devices: 30.1 us -> 0 us
  blocking collectives: 18.8 us -> 0 us
  local copies, waits for them, and re-layouts: 18.3 us -> 4.29 us
  between operations: 13.2 us -> 0.01 us
    pallas_call x0 -> x1, Pallas kernels: none -> 68.5 us  [fused(): pl.pallas_call(functools.partial(fused_kernel, sp_count, tp_count), out_s...]
    reduce_scatter x2 -> x0, waiting for transfers between devices: 50.3 us -> none  [the longest x1 31.3 us: local(): lax.psum_scatter(partial_out.reshape(tp_count, sp_count * slot_limit, D)....]
    dot_general x14 -> x0, matrix products: 34.5 us -> none  [the longest x4 10.4 us: attend_terms(): jnp.einsum('qgrd,sgd->grqs', query_grid, key_block.reshape(key_count, kv_...]
    ppermute x9 -> x0, starting transfers between devices: 25.2 us -> none  [passed_along(): lax.ppermute(value, axis, [(source, source + steps) for source in range(i...]
    another operation x5 -> x0, other arithmetic: 21.3 us -> none  [the longest x4 21.2 us: attend_terms(): lax.cumsum(keep, axis=3, reverse=True) - keep + carried[:, :, :, None]]
    all_gather x1 -> x0, waiting for transfers between devices: 20.8 us -> none  [local(): gathered = lax.all_gather(arrived, 'tp', axis=0, tiled=True)]
    all_to_all x1 -> x0, blocking collectives: 18.8 us -> none  [local(): lax.all_to_all(outgoing, 'sp', split_axis=0, concat_axis=0, tiled=True)]
    all_to_all x1 -> x0, waiting for transfers between devices: 14.3 us -> none  [local(): lax.all_to_all(expert_result, 'sp', split_axis=0, concat_axis=0, tiled=True)]
  transfers between devices with their start and end apart: 13 -> 0, of which waited for: 4 -> 0; matrix products, arithmetic and copies ran while one was open for 13% -> 0% of each run, Pallas kernels for 0% -> 0%
where the time goes in v1:
time: 73.4 us; the launch traced here: 72.8 us
  Pallas kernels  68.5 us (93%)
  local copies, waits for them, and re-layouts  4.29 us (6%)
    pallas_call x1, Pallas kernels, fused(): pl.pallas_call(functools.partial(fused_kernel, sp_count, tp_count), out_s...  68.5 us
    unnamed x3, local copies, waits for them, and re-layouts  4.29 us

profile of v1, /device:TPU:0, one launch (start us, length us, event | category | flops | bytes accessed | tf_op | source)
XLA Modules:
  0.0 72.8 jit_solution(11014545143897416460)
XLA Ops:
  0.0 1.4 %copy.14.ids_ref = s32[32,2]{1,0:T(8,128)} copy(s32[32,2]{0,1:T(2,128)} %param.21) | data formatting | bytes 512 | tf_op args[8]
  1.4 1.4 %copy.15.gates_ref = f32[32,2]{1,0:T(8,128)} copy(f32[32,2]{0,1:T(2,128)} %param.22) | data formatting | bytes 512 | tf_op args[9]
  2.7 68.5 %shard_map.127 = bf16[32,2048]{1,0:T(8,128)(2,1)} custom-call(bf16[128,512]{1,0:T(8,128)(2,1)} %q_ref.1, bf16[128,256]{1,0:T(8,128)(2,1)} %k_ref.1, bf16[128,256]{1,0:T(8,128)(2,1)} %v_ref.1, f32[4]{0:T(128)} %bias_ref.1, s32[1,128]{1,0:T(1,128)} %bitcast.3, bf16[32,2048]{1,0:T(8,128)(2,1)} %resid_ref.1, f32[1,2048]{1,0:T(1,128)} %bitcast.2, ...), custom_call_target="tpu_custom_call" | custom-call | tf_op jit(solution)/shard_map/pallas_call | solution.py:561
  71.2 1.6 %copy.17 = bf16[32,2048]{1,0:T(8,128)(2,1)} copy(bf16[32,2048]{1,0:T(8,128)(2,1)} %shard_map.127) | data formatting | bytes 262144

commit v2 on v1

--- a/solution.py
+++ b/solution.py
@@ -252,19 +252,18 @@
             device_id_type=MESH,
         )
 
+    lane_pieces = [slice(g * DH, (g + 1) * DH) for g in range(kv_local)]
+
     def passed(hop):
         right = {"sp": lax.rem(s + 1, sp_count)}
-        own = (k_ref, v_ref, doc_ref)
-        slots = (k_all, v_all, doc_all)
+        pairs = [(doc_ref if hop == 0 else doc_all.at[hop - 1], doc_all.at[hop])]
+        for own, slots in ((k_ref, k_all), (v_ref, v_all)):
+            for lanes in lane_pieces:
+                source = own.at[:, lanes] if hop == 0 else slots.at[hop - 1, :, lanes]
+                pairs.append((source, slots.at[hop, :, lanes]))
         return [
-            remote(
-                own[j] if hop == 0 else slots[j].at[hop - 1],
-                slots[j].at[hop],
-                kv_send.at[hop, j],
-                kv_recv.at[hop, j],
-                right,
-            )
-            for j in range(3)
+            remote(src, dst, kv_send.at[hop, j], kv_recv.at[hop, j], right)
+            for j, (src, dst) in enumerate(pairs)
         ]
 
     has_right = s < sp_count - 1
@@ -327,14 +326,11 @@
 
         @pl.when(s >= hop)
         def _():
-            for copy in passed(hop - 1):
+            onward = passed(hop) if hop < sp_count - 1 else None
+            for j, copy in enumerate(passed(hop - 1)):
                 copy.wait_recv()
-            if hop < sp_count - 1:
-
-                @pl.when(has_right)
-                def _():
-                    for copy in passed(hop):
-                        copy.start()
+                if onward is not None:
+                    pl.when(has_right)(onward[j].start)
 
             attend(hop)
 
@@ -343,111 +339,124 @@
             h = g * rep + r
             mixed[:, h * DH : (h + 1) * DH] = mix_acc[g, r * tok : (r + 1) * tok, :].astype(bf16)
 
-    def pair_copies(i):
+    cuts = 2
+    span = model // cuts
+    cols = [slice(h * span, (h + 1) * span) for h in range(cuts)]
+
+    def pair_copies(i, h):
         return [
             remote(
-                part.at[i, 2 * j + 1 - c],
-                sib_in.at[i, j],
-                ps_send.at[i, j],
-                ps_recv.at[i, j],
+                part.at[i, 2 * j + 1 - c, :, cols[h]],
+                sib_in.at[i, j, :, cols[h]],
+                ps_send.at[i, j, h],
+                ps_recv.at[i, j, h],
                 {"tp": sibling},
             )
             for j in range(width)
         ]
 
-    def across_copies(i):
+    def across_copies(i, h):
         return [
             remote(
-                x_out.at[i, j - 1],
-                x_in.at[i, j - 1],
-                px_send.at[i, j - 1],
-                px_recv.at[i, j - 1],
+                x_out.at[i, j - 1, :, cols[h]],
+                x_in.at[i, j - 1, :, cols[h]],
+                px_send.at[i, j - 1, h],
+                px_recv.at[i, j - 1, h],
                 {"tp": 2 * lax.rem(x + j, width) + c},
             )
             for j in range(1, width)
         ]
 
-    def pair_sum(i, at):
-        return part[i, 2 * at + c].astype(f32) + sib_in[i, at].astype(f32)
+    def pair_sum(i, at, h):
+        return part[i, 2 * at + c, :, cols[h]].astype(f32) + sib_in[i, at, :, cols[h]].astype(f32)
 
     def sum_pairs(i):
-        for copy in pair_copies(i):
+        for h in range(cuts):
+            for copy in pair_copies(i, h):
+                copy.wait_recv()
+            for j, copy in enumerate(across_copies(i, h)):
+                x_out[i, j, :, cols[h]] = pair_sum(i, lax.rem(x + j + 1, width), h).astype(bf16)
+                copy.start()
+
+    def sum_across(i, h):
+        result = pair_sum(i, x, h)
+        for j, copy in enumerate(across_copies(i, h)):
             copy.wait_recv()
-        for j, copy in enumerate(across_copies(i)):
-            x_out[i, j] = pair_sum(i, lax.rem(x + j + 1, width)).astype(bf16)
-            copy.start()
-
-    def sum_across(i):
-        result = pair_sum(i, x)
-        for j, copy in enumerate(across_copies(i)):
-            copy.wait_recv()
-            result = result + x_in[i, j].astype(f32)
+            result = result + x_in[i, j, :, cols[h]].astype(f32)
         return result
 
     loads[0].wait()
-    step = 512 if model % 512 == 0 else model
-
-    def project(n, _):
-        columns = pl.ds(pl.multiple_of(n * step, step), step)
-        value = jnp.dot(mixed[...], w_out[:, columns], preferred_element_type=f32)
-        part[sp_count, :, :, columns] = value.astype(bf16).reshape(tp_count, rows, step)
-        return 0
-
-    lax.fori_loop(0, model // step, project, 0)
-    for copy in pair_copies(sp_count):
-        copy.start()
+    step = 512 if span % 512 == 0 else span
+    steps = span // step
+
+    def into_part(i, left, right):
+        for h in range(cuts):
+
+            def piece(n, _):
+                columns = pl.ds(pl.multiple_of(n * step, step), step)
+                value = jnp.dot(left[...], right[:, columns], preferred_element_type=f32)
+                part[i, :, :, columns] = value.astype(bf16).reshape(tp_count, rows, step)
+                return 0
+
+            lax.fori_loop(h * steps, (h + 1) * steps, piece, 0)
+            for copy in pair_copies(i, h):
+                copy.start()
+
+    into_part(sp_count, mixed, w_out)
     sum_pairs(sp_count)
-    mid_value = (resid_ref[...].astype(f32) + sum_across(sp_count)).astype(bf16).astype(f32)
-    middle[...] = mid_value
+    for h in range(cuts):
+        middle[:, cols[h]] = (
+            (resid_ref[:, cols[h]].astype(f32) + sum_across(sp_count, h)).astype(bf16).astype(f32)
+        )
+    mid_value = middle[...]
     x_all[s, t] = (
         mid_value
         * lax.rsqrt(jnp.mean(mid_value * mid_value, axis=1, keepdims=True) + 1e-06)
         * gain_ref[...]
     ).astype(bf16)
 
-    def along_copy(i):
-        return remote(
-            x_all.at[s, t],
-            x_all.at[s, t],
-            z_send.at[i],
-            z_recv.at[i],
-            {"sp": paired(s, i, sp_count)},
-        )
-
-    def spread_copies(i):
-        block = x_all.at[paired(s, i, sp_count), t]
+    def group(i):
+        return paired(s, lax.rem(sp_count - i, sp_count), sp_count)
+
+    def along_copy(i, h):
+        block = x_all.at[s, t, :, cols[h]]
+        return remote(block, block, z_send.at[i, h], z_recv.at[i, h], {"sp": group(i)})
+
+    def spread_copies(i, h):
+        block = x_all.at[group(i), t, :, cols[h]]
         return [
             remote(
                 block,
                 block,
-                gx_send.at[i, j - 1],
-                gx_recv.at[i, j - 1],
+                gx_send.at[i, j - 1, h],
+                gx_recv.at[i, j - 1, h],
                 {"tp": 2 * lax.rem(x + j, width) + c},
             )
             for j in range(1, width)
         ]
 
-    def twin_copy(i, j):
-        block = x_all.at[paired(s, i, sp_count), 2 * lax.rem(x - j + width, width) + c]
-        return remote(block, block, gs_send.at[i, j], gs_recv.at[i, j], {"tp": sibling})
-
-    def spread(i):
-        for copy in spread_copies(i):
+    def twin_copy(i, j, h):
+        block = x_all.at[group(i), 2 * lax.rem(x - j + width, width) + c, :, cols[h]]
+        return remote(block, block, gs_send.at[i, j, h], gs_recv.at[i, j, h], {"tp": sibling})
+
+    def spread(i, h):
+        for copy in spread_copies(i, h):
             copy.start()
-        twin_copy(i, 0).start()
-
-    def return_copy(i):
+        twin_copy(i, 0, h).start()
+
+    def return_copy(i, h):
         return remote(
-            z_out.at[i],
-            returned.at[i],
-            rz_send.at[i],
-            rz_recv.at[i],
-            {"sp": paired(s, i, sp_count)},
-        )
-
-    spread(0)
-    for i in range(1, sp_count):
-        along_copy(i).start()
+            z_out.at[i, :, cols[h]],
+            returned.at[i, :, cols[h]],
+            rz_send.at[i, h],
+            rz_recv.at[i, h],
+            {"sp": group(i)},
+        )
+
+    for h in range(cuts):
+        for i in range(1, sp_count):
+            along_copy(i, h).start()
+        spread(0, h)
     for load in loads[1:]:
         load.wait()
 
@@ -456,17 +465,23 @@
     def turn(i, _):
         @pl.when(i + 1 < sp_count)
         def _():
-            along_copy(i + 1).wait_recv()
-            spread(i + 1)
+            for h in range(cuts):
+                along_copy(i + 1, h).wait_recv()
+                spread(i + 1, h)
 
         @pl.when(i < sp_count)
         def _():
-            for j, copy in enumerate(spread_copies(i)):
-                copy.wait_recv()
-                twin_copy(i, j + 1).start()
-            for j in range(width):
-                twin_copy(i, j).wait_recv()
-            rows_in = x_all[paired(s, i, sp_count)].reshape(tp_count * rows, model)
+            for h in range(cuts):
+                for j, copy in enumerate(spread_copies(i, h)):
+                    copy.wait_recv()
+                    twin_copy(i, j + 1, h).start()
+            for h in range(cuts):
+                for j in range(width):
+                    twin_copy(i, j, h).wait_recv()
+
+        @pl.when(i < sp_count)
+        def _():
+            rows_in = x_all[group(i)].reshape(tp_count * rows, model)
 
             def widen(n, _):
                 columns = pl.ds(pl.multiple_of(n * f_step, f_step), f_step)
@@ -476,16 +491,7 @@
                 return 0
 
             lax.fori_loop(0, ff // f_step, widen, 0)
-
-            def narrow(n, _):
-                columns = pl.ds(pl.multiple_of(n * step, step), step)
-                value = jnp.dot(hidden[...], w_down[:, columns], preferred_element_type=f32)
-                part[i, :, :, columns] = value.astype(bf16).reshape(tp_count, rows, step)
-                return 0
-
-            lax.fori_loop(0, model // step, narrow, 0)
-            for copy in pair_copies(i):
-                copy.start()
+            into_part(i, hidden, w_down)
 
         @pl.when((i >= 1) & (i <= sp_count))
         def _():
@@ -493,25 +499,29 @@
 
         @pl.when(i >= 2)
         def _():
-            z_out[i - 2] = sum_across(i - 2).astype(bf16)
-
-            @pl.when(i > 2)
-            def _():
-                return_copy(i - 2).start()
+            for h in range(cuts):
+                z_out[i - 2, :, cols[h]] = sum_across(i - 2, h).astype(bf16)
+                pl.when(i > 2)(return_copy(i - 2, h).start)
 
         return 0
 
     lax.fori_loop(0, sp_count + 2, turn, 0)
 
-    result = middle[...]
+    diagonal = lax.broadcasted_iota(jnp.int32, (rows, rows), 0) == lax.broadcasted_iota(
+        jnp.int32, (rows, rows), 1
+    )
     for i in range(sp_count):
-        if i > 0:
-            return_copy(i).wait_recv()
-        chosen = ids_ref[...] == paired(s, i, sp_count)
-        gate = jnp.sum(jnp.where(chosen, gates_ref[...], 0.0), axis=1, keepdims=True)
-        value = z_out[0] if i == 0 else returned[i]
-        result = result + gate * value.astype(f32)
-    out_ref[...] = result.astype(bf16)
+        chosen = ids_ref[...] == group(i)
+        gate_row = jnp.sum(jnp.where(chosen, gates_ref[...], 0.0), axis=0, keepdims=True)
+        gate = jnp.sum(
+            jnp.where(diagonal, jnp.broadcast_to(gate_row, (rows, rows)), 0.0), axis=1, keepdims=True
+        )
+        for h in range(cuts):
+            if i > 0:
+                return_copy(i, h).wait_recv()
+            value = z_out[0, :, cols[h]] if i == 0 else returned[i, :, cols[h]]
+            middle[:, cols[h]] = middle[:, cols[h]] + gate * value.astype(f32)
+    out_ref[...] = middle[...].astype(bf16)
 
     for hop in range(sp_count - 1):
 
@@ -520,17 +530,26 @@
             for copy in passed(hop):
                 copy.wait_send()
 
-    for i in range(sp_count + 1):
-        for copy in pair_copies(i) + across_copies(i):
-            copy.wait_send()
-    for i in range(sp_count):
-        if i > 0:
-            along_copy(i).wait_send()
-            return_copy(i).wait_send()
-        for copy in spread_copies(i):
-            copy.wait_send()
-        for j in range(width):
-            twin_copy(i, j).wait_send()
+    def drain(i, _):
+        for h in range(cuts):
+            for copy in pair_copies(i, h) + across_copies(i, h):
+                copy.wait_send()
+
+            @pl.when(i < sp_count)
+            def _():
+                for copy in spread_copies(i, h):
+                    copy.wait_send()
+                for j in range(width):
+                    twin_copy(i, j, h).wait_send()
+
+            @pl.when((i >= 1) & (i < sp_count))
+            def _():
+                along_copy(i, h).wait_send()
+                return_copy(i, h).wait_send()
+
+        return 0
+
+    lax.fori_loop(0, sp_count + 1, drain, 0)
 
 
 def fused(
@@ -587,20 +606,20 @@
             pltpu.VMEM((sp_count, rows, model), bf16),
             pltpu.VMEM((sp_count, rows, model), bf16),
             dma((4,)),
-            dma((sp_count - 1, 3)),
-            dma((sp_count - 1, 3)),
-            dma((sp_count,)),
-            dma((sp_count,)),
-            dma((sp_count, width - 1)),
-            dma((sp_count, width - 1)),
-            dma((sp_count, width)),
-            dma((sp_count, width)),
-            dma((sp_count + 1, width)),
-            dma((sp_count + 1, width)),
-            dma((sp_count + 1, width - 1)),
-            dma((sp_count + 1, width - 1)),
-            dma((sp_count,)),
-            dma((sp_count,)),
+            dma((sp_count - 1, 2 * kv_local + 1)),
+            dma((sp_count - 1, 2 * kv_local + 1)),
+            dma((sp_count, 2)),
+            dma((sp_count, 2)),
+            dma((sp_count, width - 1, 2)),
+            dma((sp_count, width - 1, 2)),
+            dma((sp_count, width, 2)),
+            dma((sp_count, width, 2)),
+            dma((sp_count + 1, width, 2)),
+            dma((sp_count + 1, width, 2)),
+            dma((sp_count + 1, width - 1, 2)),
+            dma((sp_count + 1, width - 1, 2)),
+            dma((sp_count, 2)),
+            dma((sp_count, 2)),
         ],
         compiler_params=pltpu.CompilerParams(
             collective_id=0, has_side_effects=True, vmem_limit_bytes=60 * 2**20
@@ -613,8 +632,8 @@
         documents.reshape(1, tok),
         resid,
         norm_gain.reshape(1, model),
-        expert_ids,
-        expert_gates,
+        expert_ids.T,
+        expert_gates.T,
         w_out,
         w_gate,
         w_up,

time: 73.4 us -> 67 us (0.913)
  Pallas kernels: 68.5 us -> 65.3 us
  local copies, waits for them, and re-layouts: 4.29 us -> 1.57 us
    pallas_call x1, Pallas kernels: 68.5 us -> 65.3 us  [fused(): pl.pallas_call(functools.partial(fused_kernel, sp_count, tp_count), out_s...]
    unnamed x3 -> x1, local copies, waits for them, and re-layouts: 4.29 us -> 1.57 us
where the time goes in v2:
time: 67 us; the launch traced here: 66.9 us
  Pallas kernels  65.3 us (97%)
  local copies, waits for them, and re-layouts  1.57 us (2%)
    pallas_call x1, Pallas kernels, fused(): pl.pallas_call(functools.partial(fused_kernel, sp_count, tp_count), out_s...  65.3 us
    unnamed x1, local copies, waits for them, and re-layouts  1.57 us

profile of v2, /device:TPU:0, one launch (start us, length us, event | category | flops | bytes accessed | tf_op | source)
XLA Modules:
  0.0 66.9 jit_solution(6919049264007412089)
XLA Ops:
  0.0 65.3 %shard_map.127 = bf16[32,2048]{1,0:T(8,128)(2,1)} custom-call(bf16[128,512]{1,0:T(8,128)(2,1)} %q_ref.1, bf16[128,256]{1,0:T(8,128)(2,1)} %k_ref.1, bf16[128,256]{1,0:T(8,128)(2,1)} %v_ref.1, f32[4]{0:T(128)} %bias_ref.1, s32[1,128]{1,0:T(1,128)} %bitcast.7, bf16[32,2048]{1,0:T(8,128)(2,1)} %resid_ref.1, f32[1,2048]{1,0:T(1,128)} %bitcast.4, ...), custom_call_target="tpu_custom_call" | custom-call | tf_op jit(solution)/shard_map/pallas_call | solution.py:580
  65.3 1.6 %copy.15 = bf16[32,2048]{1,0:T(8,128)(2,1)} copy(bf16[32,2048]{1,0:T(8,128)(2,1)} %shard_map.127) | data formatting | bytes 262144
